TPU v7x, 32 devices: a whole 2x2x4 slice. The times are simulated.
32 devices in a mesh: grp: 2 (over y), dp: 2 (over x), kv: 4 (over z), tp: 2 (over core).
Axes of the slice: x: 2, y: 2, z: 4, core: 2. Of those that a mesh axis runs over, the one named last changes fastest.
Arguments:
- resid: bfloat16 [12, 2048], P(('grp', 'dp'), ('kv', 'tp')), parts along dimension 0, may hold values from -7 to 7
- keys_cache: bfloat16 [12, 4096, 256], P(('grp', 'dp'), 'kv', 'tp'), parts along dimension 0, may hold values from -310 to 310
- values_cache: bfloat16 [12, 4096, 256], P(('grp', 'dp'), 'kv', 'tp'), parts along dimension 0, may hold values from -6 to 6
- gates_cache: float32 [12, 4096, 4], P(('grp', 'dp'), 'kv', 'tp'), parts along dimension 0, may hold values from -1044 to 0, as said below
- norm_gain: float32 [2048], replicated, may hold values from 0.1 to 1.9
- w_query: bfloat16 [2048, 2048], P('kv', 'tp'), may hold values from -0.125 to 0.125
- w_key: bfloat16 [2048, 256], P('kv', 'tp'), may hold values from -0.125 to 0.125
- w_value: bfloat16 [2048, 256], P('kv', 'tp'), may hold values from -0.5 to 0.5
- w_forget: bfloat16 [2048, 4], replicated, may hold values from -0.125 to 0.125
- forget_bias: float32 [4], replicated, may hold values from -3 to 1
- w_out: bfloat16 [2048, 2048], P('tp', 'kv'), may hold values from -0.5 to 0.5
- mlp_gain: float32 [2048], replicated, may hold values from 0.1 to 1.9
- w_up: bfloat16 [2048, 8192], P('kv', 'tp'), may hold values from -0.125 to 0.125
- w_down: bfloat16 [8192, 2048], P('tp', 'kv'), may hold values from -0.0625 to 0.0625
Outputs:
- next_resid: bfloat16 [12, 2048], P(('grp', 'dp'), ('kv', 'tp')), parts along dimension 0
There are 2 independent parts, one for each index of `grp`. A program takes and returns all parts, laid end to end along the dimension named above; an argument that names none is the same for every part. Nothing has to cross between parts.
Inputs may be any that keep to these rules, and one draw needn't show every extreme that they name: gates_cache[b, p, g] is the sum of the log forget gates of the cached positions after p, so it never falls along the positions and is 0 at the last one.
All inputs are finite; a program needn't handle non-finite values.
Results may differ from a plain program's by a relative error of at most 0.028.
Values may be sent and summed in bfloat16 or wider, within the bound.
No kernel may reach another device: no remote copies, remote signals or barrier semaphores. Data moves between devices by JAX's collectives and lax.ppermute only.
A program may use at most 64 MiB of HBM per device.

v0:
```python
import jax
import jax.numpy as jnp
from jax import lax
from jax.sharding import PartitionSpec as P

D = 2048
HEADS = 32
LOOKUP_GROUPS = 4
HEAD = 64


EPS = 1e-06


def joined(value, axis, join):
    pieces = jax.tree.map(lambda part: lax.all_gather(part, axis), value)
    head = jax.tree.map(lambda part: part[0], pieces)
    tail = jax.tree.map(lambda part: part[1:], pieces)
    running, _ = lax.scan(lambda running, section: (join(running, section), None), head, tail)
    return running


def prepare_rows(source, gain_vector, offset, width_block):
    own_block = lax.all_gather(source, "tp", axis=1, tiled=True).astype(jnp.float32)
    squares = jnp.sum(own_block * own_block, axis=1, keepdims=True)
    gain_block = lax.dynamic_slice_in_dim(gain_vector, offset, width_block, 0)
    scaled = (own_block * gain_block).astype(jnp.bfloat16)
    return (scaled, squares, None)


def merge_parts(earlier, later):
    peak_a, total_a, mixed_a = earlier
    peak_b, total_b, mixed_b = later
    new_peak = jnp.maximum(peak_a, peak_b)
    scale_a = jnp.exp(peak_a - new_peak)
    scale_b = jnp.exp(peak_b - new_peak)
    return (
        new_peak,
        total_a * scale_a + total_b * scale_b,
        mixed_a * scale_a[..., None] + mixed_b * scale_b[..., None],
    )


def shards(
    resid,
    keys_cache,
    values_cache,
    gates_cache,
    norm_gain,
    w_query,
    w_key,
    w_value,
    w_forget,
    forget_bias,
    w_out,
    mlp_gain,
    w_up,
    w_down,
):
    row_count = resid.shape[0]
    width_block = w_query.shape[0]
    offset = lax.axis_index("kv") * width_block
    local_heads = w_key.shape[1] // HEAD
    group_size = HEADS // LOOKUP_GROUPS
    head_offset = lax.axis_index("tp") * local_heads
    scaled, squares, inverse = prepare_rows(resid, norm_gain, offset, width_block)
    forget_rows = lax.dynamic_slice(w_forget, (offset, head_offset), (width_block, local_heads))
    query_part = jnp.dot(scaled, w_query, preferred_element_type=jnp.float32)
    key_part = jnp.dot(scaled, w_key, preferred_element_type=jnp.float32)
    value_part = jnp.dot(scaled, w_value, preferred_element_type=jnp.float32)
    forget_part = jnp.dot(scaled, forget_rows, preferred_element_type=jnp.float32)
    query_sum, key_sum, value_sum, forget_sum, norm_total = lax.psum(
        (query_part, key_part, value_part, forget_part, squares), "kv"
    )
    inverse = lax.rsqrt(norm_total / D + EPS)
    bias_local = lax.dynamic_slice_in_dim(forget_bias, head_offset, local_heads, 0)
    log_forget = jax.nn.log_sigmoid(forget_sum * inverse + bias_local)
    query = (
        (query_sum * inverse).astype(jnp.bfloat16).reshape(row_count, local_heads, group_size, HEAD)
    )
    key_new = (key_sum * inverse).astype(jnp.bfloat16).reshape(row_count, local_heads, HEAD)
    value_new = (value_sum * inverse).astype(jnp.bfloat16).reshape(row_count, local_heads, HEAD)
    ctx_len = keys_cache.shape[1]
    cached_keys = keys_cache.reshape(row_count, ctx_len, local_heads, HEAD)
    cached_values = values_cache.reshape(row_count, ctx_len, local_heads, HEAD)
    score_scale = HEAD ** (-0.5)
    scores = (
        jnp.einsum("bgjd,bpgd->bgjp", query, cached_keys, preferred_element_type=jnp.float32)
        * score_scale
    )
    gate_bias = jnp.transpose(gates_cache, (0, 2, 1)) + log_forget[:, :, None]
    scores = scores + gate_bias[:, :, None, :]
    maxima = jnp.max(scores, axis=3)
    weights = jnp.exp(scores - maxima[..., None])
    totals = jnp.sum(weights, axis=3)
    mixed = jnp.einsum(
        "bgjp,bpgd->bgjd",
        weights.astype(jnp.bfloat16),
        cached_values,
        preferred_element_type=jnp.float32,
    )
    maxima, totals, mixed = joined((maxima, totals, mixed), "kv", merge_parts)
    fresh = (
        jnp.einsum("bgjd,bgd->bgj", query, key_new, preferred_element_type=jnp.float32)
        * score_scale
    )
    new_peak = jnp.maximum(maxima, fresh)
    carried = jnp.exp(maxima - new_peak)
    own_weight = jnp.exp(fresh - new_peak)
    totals = totals * carried + own_weight
    mixed = mixed * carried[..., None] + jnp.einsum(
        "bgj,bgd->bgjd",
        own_weight.astype(jnp.bfloat16),
        value_new,
        preferred_element_type=jnp.float32,
    )
    attended = (
        (mixed / totals[..., None])
        .astype(jnp.bfloat16)
        .reshape(row_count, local_heads * group_size * HEAD)
    )
    out_part = jnp.dot(attended, w_out, preferred_element_type=jnp.float32)
    branch = lax.psum_scatter(
        out_part.astype(jnp.bfloat16), "tp", scatter_dimension=1, tiled=True
    ).astype(jnp.float32)
    middle = (resid.astype(jnp.float32) + branch).astype(jnp.bfloat16)
    scaled_mid, squares_mid, inverse_mid = prepare_rows(middle, mlp_gain, offset, width_block)
    up_part = jnp.dot(scaled_mid, w_up, preferred_element_type=jnp.float32)
    up_total, norm_mid = (
        lax.psum(up_part.astype(jnp.bfloat16), "kv").astype(jnp.float32),
        lax.psum(squares_mid.astype(jnp.bfloat16), "kv").astype(jnp.float32),
    )
    inverse_mid = lax.rsqrt(norm_mid / D + EPS)
    hidden = jnp.square(jax.nn.relu(up_total * inverse_mid)).astype(jnp.bfloat16)
    down_part = jnp.dot(hidden, w_down, preferred_element_type=jnp.float32)
    mixer_out = lax.psum_scatter(
        down_part.astype(jnp.bfloat16), "tp", scatter_dimension=1, tiled=True
    ).astype(jnp.float32)
    return (middle.astype(jnp.float32) + mixer_out).astype(jnp.bfloat16)


def solution(mesh):
    in_specs = (
        P(("grp", "dp"), ("kv", "tp")),
        P(("grp", "dp"), "kv", "tp"),
        P(("grp", "dp"), "kv", "tp"),
        P(("grp", "dp"), "kv", "tp"),
        P(),
        P("kv", "tp"),
        P("kv", "tp"),
        P("kv", "tp"),
        P(),
        P(),
        P("tp", "kv"),
        P(),
        P("kv", "tp"),
        P("tp", "kv"),
    )
    out_specs = P(("grp", "dp"), ("kv", "tp"))
    return jax.shard_map(shards, mesh=mesh, in_specs=in_specs, out_specs=out_specs, check_vma=False)
```

profile of v0, /device:TPU:0, one launch (start us, length us, event | category | flops | bytes accessed | tf_op | source)
XLA Modules:
  0.0 130.3 jit_solution(91823296636983148)
XLA Ops:
  6.5 2.2 %all_gather.24 = bf16[3,512]{1,0:T(4,128)(2,1)S(1)} all-gather(bf16[3,256]{1,0:T(4,128)(2,1)} %param.16), channel_id=1, replica_groups=mesh['grp'=2,'dp'=2,'kv'=4,'tp'=2] {'tp'}, dimensions={1}, use_global_device_ids=true | all-gather | bytes 4608 | tf_op jit(solution)/shard_map/all_gather | solution.py:24
  8.8 0.8 dynamic_slice.23
  9.5 0.1 fusion.12
  9.7 0.2 fusion.27
  9.9 1.0 fusion.28
  11.0 1.1 fusion.30
  12.0 0.9 fusion.19
  12.9 20.5 %all-reduce = (f32[3,1024]{1,0:T(4,128)S(1)}, f32[3,1]{0,1:T(1,128)S(1)}, f32[3,2]{0,1:T(2,128)S(1)}, f32[3,128]{1,0:T(4,128)S(1)}, f32[3,128]{1,0:T(4,128)S(1)}) all-reduce(f32[3,1024]{1,0:T(4,128)S(1)} %fusion.27, f32[3,1]{0,1:T(1,128)S(1)} %bitcast.69, ...), channel_id=1, replica_groups=mesh['grp'=2,'dp'=2,'kv'=4,'tp'=2] {'kv'}, use_global_device_ids=true, to_apply=%region_0.0 | all-reduce | flops 3849 | bytes 30792 | tf_op jit(solution)/shard_map/psum | solution.py:72
  33.4 0.1 multiply_convert_fusion.2
  33.5 0.1 reshape.39
  33.6 0.7 dynamic_slice.25
  34.3 0.1 fusion.22
  34.4 0.1 copy.22
  34.5 1.4 %copy.21 = bf16[3,1024,128]{1,2,0:T(8,128)(2,1)S(1)} copy(bf16[3,1024,128]{2,1,0:T(8,128)(2,1)} %param.17) | data formatting | bytes 1572864 | tf_op args[1]
  35.9 1.4 %copy.23 = bf16[3,1024,128]{1,2,0:T(8,128)(2,1)S(1)} copy(bf16[3,1024,128]{2,1,0:T(8,128)(2,1)} %param.18) | data formatting | bytes 1572864 | tf_op args[2]
  37.4 0.1 add_bitcast_fusion
  37.4 0.3 fusion.26
  37.7 0.4 fusion.6
  38.1 13.2 %all-gather.2 = f32[12,2,8,64]{3,2,1,0:T(8,128)S(1)} all-gather(f32[3,2,8,64]{3,2,1,0:T(8,128)S(1)} %fusion.6), channel_id=4, replica_groups=mesh['grp'=2,'dp'=2,'kv'=4,'tp'=2] {'kv'}, dimensions={0}, use_global_device_ids=true | all-gather | bytes 61440 | tf_op jit(solution)/shard_map/all_gather | solution.py:16
  51.4 0.2 fusion.5
  51.6 13.1 %all-gather.1 = f32[12,2,8]{2,1,0:T(2,128)S(1)} all-gather(f32[3,2,8]{2,1,0:T(2,128)S(1)} %fusion.5), channel_id=3, replica_groups=mesh['grp'=2,'dp'=2,'kv'=4,'tp'=2] {'kv'}, dimensions={0}, use_global_device_ids=true | all-gather | bytes 960 | tf_op jit(solution)/shard_map/all_gather | solution.py:16
  64.7 13.1 %all-gather = f32[12,2,8]{2,1,0:T(2,128)S(1)} all-gather(f32[3,2,8]{2,1,0:T(2,128)S(1)} %get-tuple-element.79), channel_id=2, replica_groups=mesh['grp'=2,'dp'=2,'kv'=4,'tp'=2] {'kv'}, dimensions={0}, use_global_device_ids=true | all-gather | bytes 960 | tf_op jit(solution)/shard_map/all_gather | solution.py:16
  77.8 0.4 while.14
  77.9 0.1 fusion.50
  78.0 0.1 fusion.50
  78.1 0.1 fusion.50
  78.2 0.1 fusion.21
  78.3 0.1 reshape.61
  78.4 0.1 fusion.29
  78.5 0.1 reshape.45
  78.6 0.1 divide_convert_fusion
  78.7 0.1 reshape.44
  78.8 1.5 %convolution_convert_fusion.2 = bf16[3,512]{1,0:T(4,128)(2,1)S(1)} fusion(bf16[3,1024]{1,0:T(4,128)(2,1)S(1)} %reshape.44, bf16[1024,512]{1,0:T(8,128)(2,1)} %param.26), kind=kOutput, calls=%fused_computation.12 | convolution fusion | flops 3147264 | bytes 1057792 | tf_op jit(solution)/shard_map/dot_general | solution.py:122
  80.3 0.8 copy.26
  81.1 0.0 reduce-scatter.7.cloned.1.call-update
  81.1 0.0 reduce-scatter.9.cloned.1.call-start
  81.1 0.8 dynamic_slice.26
  81.9 5.1 %reduce-scatter.7.cloned.1.call-done = bf16[256,3]{1,0:T(8,128)(2,1)} async-done(((bf16[512,3]{1,0:T(8,128)(2,1)}), bf16[256,3]{1,0:T(8,128)(2,1)}) %reduce-scatter.7.cloned.1.call-update) | async-done | bytes 1552
  87.1 0.9 copy.27
  88.0 1.8 %all_gather.31 = bf16[3,512]{1,0:T(4,128)(2,1)S(1)} all-gather(bf16[3,256]{1,0:T(4,128)(2,1)S(1)} %add_convert_fusion.1), channel_id=1, replica_groups=mesh['grp'=2,'dp'=2,'kv'=4,'tp'=2] {'tp'}, dimensions={1}, use_global_device_ids=true | all-gather | bytes 4608 | tf_op jit(solution)/shard_map/all_gather | solution.py:24
  89.8 0.1 fusion.14
  90.0 2.8 %convolution_convert_fusion = bf16[3,4096]{1,0:T(4,128)(2,1)S(1)} fusion(bf16[512,4096]{1,0:T(8,128)(2,1)} %param.28, bf16[3,512]{1,0:T(4,128)(2,1)S(1)} %all_gather.31, f32[512]{0:T(512)S(1)} %dynamic_slice.26), kind=kOutput, calls=%fused_computation.8 | convolution fusion | flops 12599808 | bytes 4224000 | tf_op jit(solution)/shard_map/dot_general | solution.py:128
  92.8 19.5 %all-reduce.1 = (bf16[3,4096]{1,0:T(4,128)(2,1)S(1)}, bf16[3,1]{0,1:T(2,128)(2,1)S(1)}) all-reduce(bf16[3,4096]{1,0:T(4,128)(2,1)S(1)} %convolution_convert_fusion, bf16[3,1]{0,1:T(2,128)(2,1)S(1)} %bitcast.68), channel_id=1, replica_groups=mesh['grp'=2,'dp'=2,'kv'=4,'tp'=2] {'kv'}, use_global_device_ids=true, to_apply=%region_11.12 | all-reduce | flops 12291 | bytes 49164 | tf_op jit(solution)/shard_map/psum | solution.py:130
  112.4 2.9 %convolution_convert_fusion.1 = bf16[3,512]{1,0:T(4,128)(2,1)S(1)} fusion(bf16[4096,512]{1,0:T(8,128)(2,1)} %param.29, bf16[3,4096]{1,0:T(4,128)(2,1)S(1)} %get-tuple-element.66, f32[3]{0:T(128)S(1)} %rsqrt_bitcast_fusion), kind=kOutput, calls=%fused_computation.11 | convolution fusion | flops 12645888 | bytes 4221964 | tf_op jit(solution)/shard_map/dot_general | solution.py:135
  115.2 0.8 copy.28
  116.1 5.9 %reduce-scatter.9.cloned.1.call-done = bf16[256,3]{1,0:T(8,128)(2,1)} async-done(((bf16[512,3]{1,0:T(8,128)(2,1)}), bf16[256,3]{1,0:T(8,128)(2,1)}) %reduce-scatter.9.cloned.1.call-update) | async-done | bytes 1552
  122.0 0.9 copy.29
  122.9 0.6 add_convert_fusion
  (21 shorter events, 0.2 us)
Async XLA Ops:
  6.5 3.1 %copy-start = (bf16[512,1024]{1,0:T(8,128)(2,1)S(1)}, bf16[512,1024]{1,0:T(8,128)(2,1)}, u32[]{:S(2)}) copy-start(bf16[512,1024]{1,0:T(8,128)(2,1)} %param.21) | copy-start | bytes 3145732
  6.5 30.8 %copy-start.1 = (f32[3,1024,2]{1,2,0:T(2,128)S(1)}, f32[3,1024,2]{1,2,0:T(2,128)}, u32[]{:S(2)}) copy-start(f32[3,1024,2]{1,2,0:T(2,128)} %param.19) | copy-start | bytes 73732
  6.5 80.5 %reduce-scatter.7.cloned.1.call-start = ((), (), s32[]{:S(2)}) async-start(), calls=%async_computation.2 | async-start | bytes 196608
  11.0 77.0 %copy-start.2 = (bf16[3,256]{1,0:T(4,128)(2,1)S(1)}, bf16[3,256]{1,0:T(4,128)(2,1)}, u32[]{:S(2)}) copy-start(bf16[3,256]{1,0:T(4,128)(2,1)} %param.16) | copy-start | bytes 4612
  81.1 40.9 %reduce-scatter.9.cloned.1.call-start = ((), (), s32[]{:S(2)}) async-start(), calls=%async_computation.3 | async-start | bytes 196608
Sparse Core Ops, SparseCore 0:
  81.2 5.7 reduce-scatter.6
  116.2 5.7 reduce-scatter.8
where the time goes:
time: 131 us; the launch traced here: 130 us
  blocking collectives  83.7 us (64%)
  between operations  13.5 us (10%)
  matrix products  11.2 us (9%)
  waiting for transfers between devices  11.1 us (8%)
  local copies, waits for them, and re-layouts  8.98 us (7%)
  other arithmetic  1.82 us (1%)
    all_gather x3, blocking collectives, joined(): pieces = jax.tree.map(lambda part: lax.all_gather(part, axis), value)  39.5 us
    psum x1, blocking collectives, shards(): lax.psum((query_part, key_part, value_part, forget_part, squares), 'kv')  20.5 us
    psum x1, blocking collectives, shards(): lax.psum(up_part.astype(jnp.bfloat16), 'kv').astype(jnp.float32)  19.5 us
    unnamed x4, waiting for transfers between devices  11.1 us
    unnamed x12, local copies, waits for them, and re-layouts  6.26 us
    all_gather x2, blocking collectives, prepare_rows(): lax.all_gather(source, 'tp', axis=1, tiled=True).astype(jnp.float32)  4.08 us
    dot_general x1, matrix products, shards(): down_part = jnp.dot(hidden, w_down, preferred_element_type=jnp.float32)  2.87 us
    dot_general x1, matrix products, shards(): up_part = jnp.dot(scaled_mid, w_up, preferred_element_type=jnp.float32)  2.84 us
  transfers between devices with their start and end apart: 2, of which 2 were waited for; matrix products, arithmetic and copies ran while one was open for 1% of the time, Pallas kernels for 0%

commit v1 on v0

v1 whole, which is shorter than its diff:
```python
import functools

import jax
import jax.numpy as jnp
from jax import lax
from jax.experimental import pallas as pl
from jax.experimental.pallas import tpu as pltpu
from jax.sharding import PartitionSpec as P

EPS = 1e-06
LANES = 128
GRANT = 12 * 1024 * 1024

F32 = jnp.float32
BF16 = jnp.bfloat16


def dot(left, right):
    return jnp.dot(left, right, preferred_element_type=F32)


def dot_t(left, right):
    return lax.dot_general(left, right, (((1,), (1,)), ((), ())), preferred_element_type=F32)


def tree_sum(parts):
    while len(parts) > 1:
        parts = [parts[k] + parts[k + 1] for k in range(0, len(parts), 2)]
    return parts[0]


def call(kernel, out, *operands, **static):
    return pl.pallas_call(
        functools.partial(kernel, **static),
        out_shape=out,
        compiler_params=pltpu.CompilerParams(vmem_limit_bytes=GRANT),
    )(*operands)


def swap(value, axis, step):
    size = lax.axis_size(axis)
    return lax.ppermute(value, axis, [(k, k ^ step) for k in range(size)])


def exchange(value, axis):
    return [value] + [swap(value, axis, step) for step in range(1, lax.axis_size(axis))]


def block_rows(own, other):
    first = lax.axis_index("tp") == 0
    own, other = own.astype(F32), other.astype(F32)
    return jnp.concatenate([jnp.where(first, own, other), jnp.where(first, other, own)], axis=1)


def project_kernel(own, other, gain, w_query, w_key, w_value, w_forget, out):
    width, qw = w_query.shape
    kw = w_key.shape[1]
    groups = w_forget.shape[0]
    offset = pl.multiple_of(lax.axis_index("kv") * width, LANES)
    rows = block_rows(own[...], other[...])
    scaled = (rows * gain[:, pl.ds(offset, width)]).astype(BF16)
    out[:, :qw] = dot(scaled, w_query[...])
    out[:, qw : qw + kw] = dot(scaled, w_key[...])
    out[:, qw + kw : qw + 2 * kw] = dot(scaled, w_value[...])
    tail = qw + 2 * kw
    out[:, tail:] = jnp.zeros((out.shape[0], LANES), F32)
    out[:, tail : tail + groups] = dot_t(scaled, w_forget[:, pl.ds(offset, width)])
    out[:, tail + groups : tail + groups + 1] = jnp.sum(rows * rows, axis=1, keepdims=True)


def attend_kernel(*refs, count, features):
    parts = refs[:count]
    keys, values, gates, bias, out = refs[count:]
    batch, _, kw = keys.shape
    local = gates.shape[1]
    groups = bias.shape[1]
    head = kw // local
    tail = parts[0].shape[1] - LANES
    qw = tail - 2 * kw
    pairs = qw // kw
    scale = head ** (-0.5)
    total = tree_sum([part[...] for part in parts])
    inverse = lax.rsqrt(total[:, tail + groups : tail + groups + 1] / features + EPS)
    query = (total[:, :qw] * inverse).astype(BF16).astype(F32)
    key_new = (total[:, qw : qw + kw] * inverse).astype(BF16).astype(F32)
    value_new = (total[:, qw + kw : tail] * inverse).astype(BF16).astype(F32)
    logit = total[:, tail : tail + groups] * inverse + bias[...]
    forget_all = jnp.minimum(logit, 0.0) - jnp.log(1.0 + jnp.exp(-jnp.abs(logit)))
    column = lax.broadcasted_iota(jnp.int32, forget_all.shape, 1) - lax.axis_index("tp") * local
    forget = [
        jnp.sum(jnp.where(column == g, forget_all, 0.0), axis=1, keepdims=True) for g in range(local)
    ]
    holds_new = lax.axis_index("kv") == 0
    low = lax.broadcasted_iota(jnp.int32, (pairs, kw), 1) < head
    first = lax.broadcasted_iota(jnp.int32, (pairs, kw), 0) < pairs // 2
    first_col = lax.broadcasted_iota(jnp.int32, (pairs, 1), 0) < pairs // 2
    lane = lax.broadcasted_iota(jnp.int32, (pairs, LANES), 1)
    stats = jnp.zeros((pairs, LANES), F32)
    for b in range(batch):
        straight = jnp.concatenate(
            [query[b : b + 1, k * kw : (k + 1) * kw] for k in range(pairs)], axis=0
        )
        rolled = pltpu.roll(straight, head, 1)
        even = jnp.where(first, jnp.where(low, straight, 0.0), jnp.where(low, 0.0, rolled))
        odd = jnp.where(first, jnp.where(low, rolled, 0.0), jnp.where(low, 0.0, straight))
        heads = jnp.concatenate([even, odd], axis=0)
        gate = jnp.where(first_col, gates[b, 0:1, :], gates[b, 1:2, :])
        scores = dot_t(heads.astype(BF16), keys[b]) * scale + jnp.concatenate([gate, gate], axis=0)
        decay = jnp.where(first_col, forget[0][b : b + 1], forget[1][b : b + 1])
        decay = jnp.concatenate([decay, decay], axis=0)
        fresh = jnp.sum(heads * key_new[b : b + 1], axis=1, keepdims=True) * scale
        fresh = jnp.where(holds_new, fresh, -jnp.inf)
        peak = jnp.maximum(jnp.max(scores, axis=1, keepdims=True) + decay, fresh)
        weights = jnp.exp(scores + (decay - peak))
        own = jnp.exp(fresh - peak)
        sums = jnp.sum(weights, axis=1, keepdims=True) + own
        mixed = dot(weights.astype(BF16), values[b])
        mixed = mixed + own.astype(BF16).astype(F32) * value_new[b : b + 1]
        even, odd = mixed[:pairs], mixed[pairs:]
        turned_even, turned_odd = pltpu.roll(even, head, 1), pltpu.roll(odd, head, 1)
        out[b * pairs : (b + 1) * pairs, :] = jnp.where(
            low, jnp.where(first, even, turned_even), jnp.where(first, turned_odd, odd)
        )
        for parity in range(2):
            cut = slice(parity * pairs, (parity + 1) * pairs)
            stats = jnp.where(lane == 2 * b + parity, peak[cut], stats)
            stats = jnp.where(lane == LANES // 2 + 2 * b + parity, sums[cut], stats)
    out[batch * pairs :, :] = stats


def output_kernel(*refs, count, batch):
    parts = [part[...] for part in refs[:count]]
    w_out, out = refs[count:]
    pairs = parts[0].shape[0] // (batch + 1)
    kw = parts[0].shape[1]
    stats = [part[batch * pairs :] for part in parts]
    peak = functools.reduce(jnp.maximum, stats)
    factors = [jnp.exp(stat - peak) for stat in stats]
    sums = tree_sum([pltpu.roll(s, LANES // 2, 1) * f for s, f in zip(stats, factors)])
    low = lax.broadcasted_iota(jnp.int32, (pairs, kw), 1) < kw // 2
    attended = []
    for b in range(batch):
        spread = lambda tile: jnp.where(
            low, tile[:, 2 * b : 2 * b + 1], tile[:, 2 * b + 1 : 2 * b + 2]
        )
        mixed = tree_sum(
            [p[b * pairs : (b + 1) * pairs] * spread(f) for p, f in zip(parts, factors)]
        )
        attended.append(mixed / spread(sums))
    rows = jnp.concatenate(
        [
            jnp.concatenate([tile[k : k + 1] for tile in attended], axis=0) for k in range(pairs)
        ],
        axis=1,
    ).astype(BF16)
    out[...] = dot(rows, w_out[...]).astype(BF16)


def up_kernel(own, other, part, part_other, gain, w_up, out, middle_out):
    width, ff = w_up.shape
    half = own.shape[1]
    offset = pl.multiple_of(lax.axis_index("kv") * width, LANES)
    branch = part[...].astype(F32) + part_other[...].astype(F32)
    middle = (block_rows(own[...], other[...]) + branch).astype(BF16).astype(F32)
    scaled = (middle * gain[:, pl.ds(offset, width)]).astype(BF16)
    out[:, :ff] = dot(scaled, w_up[...]).astype(BF16)
    squares = jnp.sum(middle * middle, axis=1, keepdims=True)
    coarse = squares.astype(BF16).astype(F32)
    lane = lax.broadcasted_iota(jnp.int32, (out.shape[0], LANES), 1)
    pair = jnp.where(lane == 0, coarse, jnp.where(lane == 1, squares - coarse, 0.0))
    out[:, ff:] = pair.astype(BF16)
    first = lax.axis_index("tp") == 0
    middle_out[...] = jnp.where(first, middle[:, :half], middle[:, half:])


def down_kernel(*refs, count, features):
    parts = refs[:count]
    w_down, sent, kept = refs[count:]
    ff = w_down.shape[0]
    half = sent.shape[1]
    total = tree_sum([part[...].astype(F32) for part in parts])
    squares = total[:, ff : ff + 1] + total[:, ff + 1 : ff + 2]
    inverse = lax.rsqrt(squares / features + EPS)
    hidden = jnp.square(jnp.maximum(total[:, :ff] * inverse, 0.0)).astype(BF16)
    down = dot(hidden, w_down[...])
    first = lax.axis_index("tp") == 0
    sent[...] = jnp.where(first, down[:, half:], down[:, :half]).astype(BF16)
    kept[...] = jnp.where(first, down[:, :half], down[:, half:]).astype(BF16)


def shards(
    resid,
    keys_cache,
    values_cache,
    gates_cache,
    norm_gain,
    w_query,
    w_key,
    w_value,
    w_forget,
    forget_bias,
    w_out,
    mlp_gain,
    w_up,
    w_down,
):
    batch, half = resid.shape
    count = lax.axis_size("kv")
    features = norm_gain.shape[0]
    qw, kw, ff = w_query.shape[1], w_key.shape[1], w_up.shape[1]
    other = swap(resid, "tp", 1)
    packed = call(
        project_kernel,
        jax.ShapeDtypeStruct((batch, qw + 2 * kw + LANES), F32),
        resid,
        other,
        norm_gain[None, :],
        w_query,
        w_key,
        w_value,
        w_forget.T,
    )
    packed = call(
        attend_kernel,
        jax.ShapeDtypeStruct(((batch + 1) * (qw // kw), kw), F32),
        *exchange(packed, "kv"),
        keys_cache,
        values_cache,
        jnp.transpose(gates_cache, (0, 2, 1)),
        forget_bias[None, :],
        count=count,
        features=features,
    )
    part = call(
        output_kernel,
        jax.ShapeDtypeStruct((batch, w_out.shape[1]), BF16),
        *exchange(packed, "kv"),
        w_out,
        count=count,
        batch=batch,
    )
    packed, middle = call(
        up_kernel,
        (
            jax.ShapeDtypeStruct((batch, ff + LANES), BF16),
            jax.ShapeDtypeStruct((batch, half), F32),
        ),
        resid,
        other,
        part,
        swap(part, "tp", 1),
        mlp_gain[None, :],
        w_up,
    )
    sent, kept = call(
        down_kernel,
        (jax.ShapeDtypeStruct((batch, half), BF16), jax.ShapeDtypeStruct((batch, half), BF16)),
        *exchange(packed, "kv"),
        w_down,
        count=count,
        features=features,
    )
    mixer = kept.astype(F32) + swap(sent, "tp", 1).astype(F32)
    return (middle + mixer).astype(BF16)


def solution(mesh):
    in_specs = (
        P(("grp", "dp"), ("kv", "tp")),
        P(("grp", "dp"), "kv", "tp"),
        P(("grp", "dp"), "kv", "tp"),
        P(("grp", "dp"), "kv", "tp"),
        P(),
        P("kv", "tp"),
        P("kv", "tp"),
        P("kv", "tp"),
        P(),
        P(),
        P("tp", "kv"),
        P(),
        P("kv", "tp"),
        P("tp", "kv"),
    )
    out_specs = P(("grp", "dp"), ("kv", "tp"))
    return jax.shard_map(shards, mesh=mesh, in_specs=in_specs, out_specs=out_specs, check_vma=False)
```

time: 131 us -> 44.3 us (0.34)
  blocking collectives: 83.7 us -> 0 us
  starting transfers between devices: 0.04 us -> 15 us
  between operations: 13.5 us -> 0.03 us
  matrix products: 11.2 us -> 0 us
  Pallas kernels: 0 us -> 3.49 us
  local copies, waits for them, and re-layouts: 8.98 us -> 12.2 us
  waiting for transfers between devices: 11.1 us -> 12.5 us
    all_gather x5 -> x0, blocking collectives: 43.6 us -> none  [the longest x3 39.5 us: joined(): pieces = jax.tree.map(lambda part: lax.all_gather(part, axis), value)]
    psum x2 -> x0, blocking collectives: 40.1 us -> none  [the longest x1 20.5 us: shards(): lax.psum((query_part, key_part, value_part, forget_part, squares), 'kv')]
    ppermute x0 -> x12, starting transfers between devices: none -> 15 us  [swap(): return lax.ppermute(value, axis, [(k, k ^ step) for k in range(size)])]
    ppermute x0 -> x12, waiting for transfers between devices: none -> 12.5 us  [swap(): return lax.ppermute(value, axis, [(k, k ^ step) for k in range(size)])]
    dot_general x10 -> x0, matrix products: 11.2 us -> none  [the longest x1 2.87 us: shards(): down_part = jnp.dot(hidden, w_down, preferred_element_type=jnp.float32)]
    unnamed x4 -> x0, waiting for transfers between devices: 11.1 us -> none
    unnamed x12 -> x30, local copies, waits for them, and re-layouts: 6.26 us -> 12.2 us
    pallas_call x0 -> x5, Pallas kernels: none -> 3.49 us  [call(): pl.pallas_call(functools.partial(kernel, **static), out_shape=out, compil...]
  transfers between devices with their start and end apart: 2 -> 12, of which waited for: 2 -> 11; matrix products, arithmetic and copies ran while one was open for 1% -> 0% of each run, Pallas kernels for 0% -> 0%
where the time goes in v1:
time: 44.3 us; the launch traced here: 43.8 us
  starting transfers between devices  15 us (34%)
  waiting for transfers between devices  12.5 us (28%)
  local copies, waits for them, and re-layouts  12.2 us (28%)
  Pallas kernels  3.49 us (8%)
  other arithmetic  0.58 us (1%)
    ppermute x12, starting transfers between devices, swap(): return lax.ppermute(value, axis, [(k, k ^ step) for k in range(size)])  15 us
    ppermute x12, waiting for transfers between devices, swap(): return lax.ppermute(value, axis, [(k, k ^ step) for k in range(size)])  12.5 us
    unnamed x30, local copies, waits for them, and re-layouts  12.2 us
    pallas_call x5, Pallas kernels, call(): pl.pallas_call(functools.partial(kernel, **static), out_shape=out, compil...  3.49 us
  transfers between devices with their start and end apart: 12, of which 11 were waited for; matrix products, arithmetic and copies ran while one was open for 0% of the time, Pallas kernels for 0%

profile of v1, /device:TPU:0, one launch (start us, length us, event | category | flops | bytes accessed | tf_op | source)
XLA Modules:
  0.0 43.8 jit_solution(15313470972259775323)
XLA Ops:
  0.0 0.0 copy-start.11
  0.0 0.5 %collective-permute-start = (bf16[3,256]{1,0:T(4,128)(2,1)}, bf16[3,256]{1,0:T(4,128)(2,1)S(1)}, u32[]{:S(2)}, u32[]{:S(2)}) collective-permute-start(bf16[3,256]{1,0:T(4,128)(2,1)} %own.3), channel_id=1, source_target_pairs={{0,1},{1,0},{2,3},{3,2},{4,5},{5,4},{6,7},{7,6},{8,9},{9,8},{10,11... | collective-permute-start | bytes 4616 | tf_op jit(solution)/shard_map/ppermute | solution.py:42
  0.5 1.0 %collective-permute-done.other = bf16[3,256]{1,0:T(4,128)(2,1)S(1)} collective-permute-done((bf16[3,256]{1,0:T(4,128)(2,1)}, bf16[3,256]{1,0:T(4,128)(2,1)S(1)}, u32[]{:S(2)}, u32[]{:S(2)}) %collective-permute-start) | collective-permute-done | bytes 1568 | tf_op jit(solution)/shard_map/ppermute | solution.py:42
  1.5 0.0 copy-start.2
  1.5 1.2 %copy-done.2 = bf16[512,1024]{1,0:T(8,128)(2,1)S(1)} copy-done((bf16[512,1024]{1,0:T(8,128)(2,1)S(1)}, bf16[512,1024]{1,0:T(8,128)(2,1)}, u32[]{:S(2)}) %copy-start.2) | copy-done | bytes 1048600
  2.8 0.0 copy-start.6
  2.8 0.9 %copy-done.6 = bf16[512,128]{1,0:T(8,128)(2,1)S(1)} copy-done((bf16[512,128]{1,0:T(8,128)(2,1)S(1)}, bf16[512,128]{1,0:T(8,128)(2,1)}, u32[]{:S(2)}) %copy-start.6) | copy-done | bytes 131096
  3.7 0.9 %copy-done.7 = bf16[512,128]{1,0:T(8,128)(2,1)S(1)} copy-done((bf16[512,128]{1,0:T(8,128)(2,1)S(1)}, bf16[512,128]{1,0:T(8,128)(2,1)}, u32[]{:S(2)}) %copy-start.7) | copy-done | bytes 131096
  4.6 0.7 %copy-done.9 = bf16[2048,4]{0,1:T(4,128)(2,1)S(1)} copy-done((bf16[2048,4]{0,1:T(4,128)(2,1)S(1)}, bf16[2048,4]{0,1:T(4,128)(2,1)}, u32[]{:S(2)}) %copy-start.9) | copy-done | bytes 16408
  5.3 0.7 %copy-done.10 = bf16[3,256]{1,0:T(4,128)(2,1)S(1)} copy-done((bf16[3,256]{1,0:T(4,128)(2,1)S(1)}, bf16[3,256]{1,0:T(4,128)(2,1)}, u32[]{:S(2)}) %copy-start.10) | copy-done | bytes 1560
  6.0 0.7 %copy-done.12 = f32[2048]{0:T(1024)S(1)} copy-done((f32[2048]{0:T(1024)S(1)}, f32[2048]{0:T(1024)}, u32[]{:S(2)}) %copy-start.12) | copy-done | bytes 8216
  6.7 0.3 shard_map.136.refs_0_
  6.9 5.0 %collective-permute-start.3 = (f32[3,1408]{1,0:T(4,128)S(1)}, f32[3,1408]{1,0:T(4,128)S(1)}, u32[]{:S(2)}, u32[]{:S(2)}) collective-permute-start(f32[3,1408]{1,0:T(4,128)S(1)} %shard_map.136.refs_0_), channel_id=1, source_target_pairs={{0,6},{2,4},{4,2},{6,0},{1,7},{3,5},{5,3},{7,1},{8,14},{10,12},{12... | collective-permute-start | bytes 50696 | tf_op jit(solution)/shard_map/ppermute | solution.py:42
  11.9 0.0 collective-permute-start.2
  11.9 0.6 %collective-permute-start.1 = (f32[3,1408]{1,0:T(4,128)S(1)}, f32[3,1408]{1,0:T(4,128)S(1)}, u32[]{:S(2)}, u32[]{:S(2)}) collective-permute-start(f32[3,1408]{1,0:T(4,128)S(1)} %shard_map.136.refs_0_), channel_id=1, source_target_pairs={{0,2},{2,0},{4,6},{6,4},{1,3},{3,1},{5,7},{7,5},{8,10},{10,8},{12,... | collective-permute-start | bytes 50696 | tf_op jit(solution)/shard_map/ppermute | solution.py:42
  12.6 1.1 %collective-permute-done.3.refs_3_ = f32[3,1408]{1,0:T(4,128)S(1)} collective-permute-done((f32[3,1408]{1,0:T(4,128)S(1)}, f32[3,1408]{1,0:T(4,128)S(1)}, u32[]{:S(2)}, u32[]{:S(2)}) %collective-permute-start.3) | collective-permute-done | bytes 16928 | tf_op jit(solution)/shard_map/ppermute | solution.py:42
  13.7 2.9 %collective-permute-done.2.refs_2_ = f32[3,1408]{1,0:T(4,128)S(1)} collective-permute-done((f32[3,1408]{1,0:T(4,128)S(1)}, f32[3,1408]{1,0:T(4,128)S(1)}, u32[]{:S(2)}, u32[]{:S(2)}) %collective-permute-start.2) | collective-permute-done | bytes 16928 | tf_op jit(solution)/shard_map/ppermute | solution.py:42
  16.6 0.0 collective-permute-done.1.refs_1_
  16.6 1.1 %copy-done.4 = bf16[3,1024,128]{2,1,0:T(8,128)(2,1)S(1)} copy-done((bf16[3,1024,128]{2,1,0:T(8,128)(2,1)S(1)}, bf16[3,1024,128]{2,1,0:T(8,128)(2,1)}, u32[]{:S(2)}) %copy-start.4) | copy-done | bytes 786456
  17.8 1.1 %copy-done.5 = bf16[3,1024,128]{2,1,0:T(8,128)(2,1)S(1)} copy-done((bf16[3,1024,128]{2,1,0:T(8,128)(2,1)S(1)}, bf16[3,1024,128]{2,1,0:T(8,128)(2,1)}, u32[]{:S(2)}) %copy-start.5) | copy-done | bytes 786456
  18.9 0.7 %copy-done.8 = f32[3,1024,2]{1,2,0:T(2,128)S(1)} copy-done((f32[3,1024,2]{1,2,0:T(2,128)S(1)}, f32[3,1024,2]{1,2,0:T(2,128)}, u32[]{:S(2)}) %copy-start.8) | copy-done | bytes 24600
  19.6 0.7 %copy-done.14 = f32[4]{0:T(128)S(1)} copy-done((f32[4]{0:T(128)S(1)}, f32[4]{0:T(128)}, u32[]{:S(2)}) %copy-start.14) | copy-done | bytes 40
  20.3 1.4 %shard_map.137.refs_0_ = f32[32,128]{1,0:T(8,128)S(1)} custom-call(f32[3,1408]{1,0:T(4,128)S(1)} %shard_map.136.refs_0_, f32[3,1408]{1,0:T(4,128)S(1)} %collective-permute-done.1.refs_1_, f32[3,1408]{1,0:T(4,128)S(1)} %collective-permute-done.2.refs_2_, f32[3,1408]{1,0:T(4,128)S(1)} %collective-permute-done.3.refs_3_, bf16[3,1024,128]{2,1,0:T(8,128)(2,1)S(1)} %copy-done.4, ...), custom_call_target="tpu_custom_call" | custom-call | tf_op jit(solution)/shard_map/pallas_call | solution.py:33
  21.7 1.5 %collective-permute-start.6 = (f32[32,128]{1,0:T(8,128)S(1)}, f32[32,128]{1,0:T(8,128)S(1)}, u32[]{:S(2)}, u32[]{:S(2)}) collective-permute-start(f32[32,128]{1,0:T(8,128)S(1)} %shard_map.137.refs_0_), channel_id=1, source_target_pairs={{0,6},{2,4},{4,2},{6,0},{1,7},{3,5},{5,3},{7,1},{8,14},{10,12},{12... | collective-permute-start | bytes 49160 | tf_op jit(solution)/shard_map/ppermute | solution.py:42
  23.2 0.6 %collective-permute-start.5 = (f32[32,128]{1,0:T(8,128)S(1)}, f32[32,128]{1,0:T(8,128)S(1)}, u32[]{:S(2)}, u32[]{:S(2)}) collective-permute-start(f32[32,128]{1,0:T(8,128)S(1)} %shard_map.137.refs_0_), channel_id=1, source_target_pairs={{0,4},{2,6},{4,0},{6,2},{1,5},{3,7},{5,1},{7,3},{8,12},{10,14},{12... | collective-permute-start | bytes 49160 | tf_op jit(solution)/shard_map/ppermute | solution.py:42
  23.9 2.3 %collective-permute-start.4 = (f32[32,128]{1,0:T(8,128)S(1)}, f32[32,128]{1,0:T(8,128)S(1)}, u32[]{:S(2)}, u32[]{:S(2)}) collective-permute-start(f32[32,128]{1,0:T(8,128)S(1)} %shard_map.137.refs_0_), channel_id=1, source_target_pairs={{0,2},{2,0},{4,6},{6,4},{1,3},{3,1},{5,7},{7,5},{8,10},{10,8},{12,... | collective-permute-start | bytes 49160 | tf_op jit(solution)/shard_map/ppermute | solution.py:42
  26.2 1.1 %collective-permute-done.6.refs_3_ = f32[32,128]{1,0:T(8,128)S(1)} collective-permute-done((f32[32,128]{1,0:T(8,128)S(1)}, f32[32,128]{1,0:T(8,128)S(1)}, u32[]{:S(2)}, u32[]{:S(2)}) %collective-permute-start.6) | collective-permute-done | bytes 16416 | tf_op jit(solution)/shard_map/ppermute | solution.py:42
  27.3 0.6 %collective-permute-done.5.refs_2_ = f32[32,128]{1,0:T(8,128)S(1)} collective-permute-done((f32[32,128]{1,0:T(8,128)S(1)}, f32[32,128]{1,0:T(8,128)S(1)}, u32[]{:S(2)}, u32[]{:S(2)}) %collective-permute-start.5) | collective-permute-done | bytes 16416 | tf_op jit(solution)/shard_map/ppermute | solution.py:42
  27.9 0.2 collective-permute-done.4.refs_1_
  28.0 1.2 %copy-done.3 = bf16[1024,512]{1,0:T(8,128)(2,1)S(1)} copy-done((bf16[1024,512]{1,0:T(8,128)(2,1)S(1)}, bf16[1024,512]{1,0:T(8,128)(2,1)}, u32[]{:S(2)}) %copy-start.3) | copy-done | bytes 1048600
  29.3 0.4 shard_map.138.part
  29.6 0.0 collective-permute-start.7
  29.6 1.2 %collective-permute-done.7.part_other = bf16[3,512]{1,0:T(4,128)(2,1)S(1)} collective-permute-done((bf16[3,512]{1,0:T(4,128)(2,1)S(1)}, bf16[3,512]{1,0:T(4,128)(2,1)S(1)}, u32[]{:S(2)}, u32[]{:S(2)}) %collective-permute-start.7) | collective-permute-done | bytes 3104 | tf_op jit(solution)/shard_map/ppermute | solution.py:42
  30.8 0.0 copy-done.11
  30.8 0.0 copy-done.13
  30.8 2.2 %copy-done = bf16[512,4096]{1,0:T(8,128)(2,1)S(1)} copy-done((bf16[512,4096]{1,0:T(8,128)(2,1)S(1)}, bf16[512,4096]{1,0:T(8,128)(2,1)}, u32[]{:S(2)}) %copy-start) | copy-done | bytes 4194328
  33.0 0.6 %shard_map.139 = (bf16[3,4224]{1,0:T(4,128)(2,1)S(1)}, f32[3,256]{1,0:T(4,128)S(1)}) custom-call(bf16[3,256]{1,0:T(4,128)(2,1)S(1)} %copy-done.11, bf16[3,256]{1,0:T(4,128)(2,1)S(1)} %collective-permute-done.other, bf16[3,512]{1,0:T(4,128)(2,1)S(1)} %shard_map.138.part, bf16[3,512]{1,0:T(4,128)(2,1)S(1)} %collective-permute-done.7.part_other, ...), custom_call_target="tpu_custom_call" | custom-call | tf_op jit(solution)/shard_map/pallas_call | solution.py:33
  33.7 2.4 %collective-permute-start.10 = (bf16[3,4224]{1,0:T(4,128)(2,1)S(1)}, bf16[3,4224]{1,0:T(4,128)(2,1)S(1)}, u32[]{:S(2)}, u32[]{:S(2)}) collective-permute-start(bf16[3,4224]{1,0:T(4,128)(2,1)S(1)} %get-tuple-element.10.refs_0_), channel_id=1, source_target_pairs={{0,6},{2,4},{4,2},{6,0},{1,7},{3,5},{5,3},{7,1},{8,14},{10,12},{12... | collective-permute-start | bytes 76040 | tf_op jit(solution)/shard_map/ppermute | solution.py:42
  36.1 0.9 %collective-permute-start.9 = (bf16[3,4224]{1,0:T(4,128)(2,1)S(1)}, bf16[3,4224]{1,0:T(4,128)(2,1)S(1)}, u32[]{:S(2)}, u32[]{:S(2)}) collective-permute-start(bf16[3,4224]{1,0:T(4,128)(2,1)S(1)} %get-tuple-element.10.refs_0_), channel_id=1, source_target_pairs={{0,4},{2,6},{4,0},{6,2},{1,5},{3,7},{5,1},{7,3},{8,12},{10,14},{12... | collective-permute-start | bytes 76040 | tf_op jit(solution)/shard_map/ppermute | solution.py:42
  37.0 1.1 %collective-permute-start.8 = (bf16[3,4224]{1,0:T(4,128)(2,1)S(1)}, bf16[3,4224]{1,0:T(4,128)(2,1)S(1)}, u32[]{:S(2)}, u32[]{:S(2)}) collective-permute-start(bf16[3,4224]{1,0:T(4,128)(2,1)S(1)} %get-tuple-element.10.refs_0_), channel_id=1, source_target_pairs={{0,2},{2,0},{4,6},{6,4},{1,3},{3,1},{5,7},{7,5},{8,10},{10,8},{12,... | collective-permute-start | bytes 76040 | tf_op jit(solution)/shard_map/ppermute | solution.py:42
  38.1 1.7 %collective-permute-done.10.refs_3_ = bf16[3,4224]{1,0:T(4,128)(2,1)S(1)} collective-permute-done((bf16[3,4224]{1,0:T(4,128)(2,1)S(1)}, bf16[3,4224]{1,0:T(4,128)(2,1)S(1)}, u32[]{:S(2)}, u32[]{:S(2)}) %collective-permute-start.10) | collective-permute-done | bytes 25376 | tf_op jit(solution)/shard_map/ppermute | solution.py:42
  39.7 1.2 %collective-permute-done.9.refs_2_ = bf16[3,4224]{1,0:T(4,128)(2,1)S(1)} collective-permute-done((bf16[3,4224]{1,0:T(4,128)(2,1)S(1)}, bf16[3,4224]{1,0:T(4,128)(2,1)S(1)}, u32[]{:S(2)}, u32[]{:S(2)}) %collective-permute-start.9) | collective-permute-done | bytes 25376 | tf_op jit(solution)/shard_map/ppermute | solution.py:42
  40.9 0.4 collective-permute-done.8.refs_1_
  41.3 0.0 copy-done.1
  41.3 0.8 %shard_map.140 = (bf16[3,256]{1,0:T(4,128)(2,1)S(1)}, bf16[3,256]{1,0:T(4,128)(2,1)S(1)}) custom-call(bf16[3,4224]{1,0:T(4,128)(2,1)S(1)} %get-tuple-element.10.refs_0_, bf16[3,4224]{1,0:T(4,128)(2,1)S(1)} %collective-permute-done.8.refs_1_, bf16[3,4224]{1,0:T(4,128)(2,1)S(1)} %collective-permute-done.9.refs_2_, ...), custom_call_target="tpu_custom_call" | custom-call | tf_op jit(solution)/shard_map/pallas_call | solution.py:33
  42.1 0.0 collective-permute-start.11
  42.1 1.2 %collective-permute-done.11 = bf16[3,256]{1,0:T(4,128)(2,1)S(1)} collective-permute-done((bf16[3,256]{1,0:T(4,128)(2,1)S(1)}, bf16[3,256]{1,0:T(4,128)(2,1)S(1)}, u32[]{:S(2)}, u32[]{:S(2)}) %collective-permute-start.11) | collective-permute-done | bytes 1568 | tf_op jit(solution)/shard_map/ppermute | solution.py:42
  43.2 0.6 %add_convert_fusion = bf16[3,256]{1,0:T(4,128)(2,1)} fusion(f32[3,256]{1,0:T(4,128)S(1)} %get-tuple-element.9, bf16[3,256]{1,0:T(4,128)(2,1)S(1)} %collective-permute-done.11, bf16[3,256]{1,0:T(4,128)(2,1)S(1)} %get-tuple-element.11), kind=kLoop, calls=%fused_computation | loop fusion | flops 3840 | bytes 7680 | tf_op jit(solution)/shard_map/convert_element_type | solution.py:264
  (12 shorter events, 0.0 us)
Async XLA Ops:
  0.0 30.8 %copy-start.11 = (bf16[3,256]{1,0:T(4,128)(2,1)S(1)}, bf16[3,256]{1,0:T(4,128)(2,1)}, u32[]{:S(2)}) copy-start(bf16[3,256]{1,0:T(4,128)(2,1)} %own.3) | copy-start | bytes 4612
  0.0 1.5 %collective-permute-start = (bf16[3,256]{1,0:T(4,128)(2,1)}, bf16[3,256]{1,0:T(4,128)(2,1)S(1)}, u32[]{:S(2)}, u32[]{:S(2)}) collective-permute-start(bf16[3,256]{1,0:T(4,128)(2,1)} %own.3), channel_id=1, source_target_pairs={{0,1},{1,0},{2,3},{3,2},{4,5},{5,4},{6,7},{7,6},{8,9},{9,8},{10,11... | collective-permute-start | bytes 4616 | tf_op jit(solution)/shard_map/ppermute | solution.py:42
  1.5 1.2 %copy-start.2 = (bf16[512,1024]{1,0:T(8,128)(2,1)S(1)}, bf16[512,1024]{1,0:T(8,128)(2,1)}, u32[]{:S(2)}) copy-start(bf16[512,1024]{1,0:T(8,128)(2,1)} %w_query.1) | copy-start | bytes 3145732
  2.8 0.9 %copy-start.6 = (bf16[512,128]{1,0:T(8,128)(2,1)S(1)}, bf16[512,128]{1,0:T(8,128)(2,1)}, u32[]{:S(2)}) copy-start(bf16[512,128]{1,0:T(8,128)(2,1)} %w_key.1) | copy-start | bytes 393220
  3.7 0.9 %copy-start.7 = (bf16[512,128]{1,0:T(8,128)(2,1)S(1)}, bf16[512,128]{1,0:T(8,128)(2,1)}, u32[]{:S(2)}) copy-start(bf16[512,128]{1,0:T(8,128)(2,1)} %w_value.1) | copy-start | bytes 393220
  4.6 0.7 %copy-start.9 = (bf16[2048,4]{0,1:T(4,128)(2,1)S(1)}, bf16[2048,4]{0,1:T(4,128)(2,1)}, u32[]{:S(2)}) copy-start(bf16[2048,4]{0,1:T(4,128)(2,1)} %param.22) | copy-start | bytes 49156
  5.3 0.7 %copy-start.10 = (bf16[3,256]{1,0:T(4,128)(2,1)S(1)}, bf16[3,256]{1,0:T(4,128)(2,1)}, u32[]{:S(2)}) copy-start(bf16[3,256]{1,0:T(4,128)(2,1)} %own.3) | copy-start | bytes 4612
  6.0 0.7 %copy-start.12 = (f32[2048]{0:T(1024)S(1)}, f32[2048]{0:T(1024)}, u32[]{:S(2)}) copy-start(f32[2048]{0:T(1024)} %param.18) | copy-start | bytes 24580
  6.7 24.2 %copy-start.13 = (f32[2048]{0:T(1024)S(1)}, f32[2048]{0:T(1024)}, u32[]{:S(2)}) copy-start(f32[2048]{0:T(1024)} %param.25) | copy-start | bytes 24580
  6.9 6.8 %collective-permute-start.3 = (f32[3,1408]{1,0:T(4,128)S(1)}, f32[3,1408]{1,0:T(4,128)S(1)}, u32[]{:S(2)}, u32[]{:S(2)}) collective-permute-start(f32[3,1408]{1,0:T(4,128)S(1)} %shard_map.136.refs_0_), channel_id=1, source_target_pairs={{0,6},{2,4},{4,2},{6,0},{1,7},{3,5},{5,3},{7,1},{8,14},{10,12},{12... | collective-permute-start | bytes 50696 | tf_op jit(solution)/shard_map/ppermute | solution.py:42
  11.9 4.7 %collective-permute-start.2 = (f32[3,1408]{1,0:T(4,128)S(1)}, f32[3,1408]{1,0:T(4,128)S(1)}, u32[]{:S(2)}, u32[]{:S(2)}) collective-permute-start(f32[3,1408]{1,0:T(4,128)S(1)} %shard_map.136.refs_0_), channel_id=1, source_target_pairs={{0,4},{2,6},{4,0},{6,2},{1,5},{3,7},{5,1},{7,3},{8,12},{10,14},{12... | collective-permute-start | bytes 50696 | tf_op jit(solution)/shard_map/ppermute | solution.py:42
  11.9 4.7 %collective-permute-start.1 = (f32[3,1408]{1,0:T(4,128)S(1)}, f32[3,1408]{1,0:T(4,128)S(1)}, u32[]{:S(2)}, u32[]{:S(2)}) collective-permute-start(f32[3,1408]{1,0:T(4,128)S(1)} %shard_map.136.refs_0_), channel_id=1, source_target_pairs={{0,2},{2,0},{4,6},{6,4},{1,3},{3,1},{5,7},{7,5},{8,10},{10,8},{12,... | collective-permute-start | bytes 50696 | tf_op jit(solution)/shard_map/ppermute | solution.py:42
  16.6 1.1 %copy-start.4 = (bf16[3,1024,128]{2,1,0:T(8,128)(2,1)S(1)}, bf16[3,1024,128]{2,1,0:T(8,128)(2,1)}, u32[]{:S(2)}) copy-start(bf16[3,1024,128]{2,1,0:T(8,128)(2,1)} %refs_4_.3) | copy-start | bytes 2359300
  17.8 1.1 %copy-start.5 = (bf16[3,1024,128]{2,1,0:T(8,128)(2,1)S(1)}, bf16[3,1024,128]{2,1,0:T(8,128)(2,1)}, u32[]{:S(2)}) copy-start(bf16[3,1024,128]{2,1,0:T(8,128)(2,1)} %refs_5_.1) | copy-start | bytes 2359300
  18.9 0.7 %copy-start.8 = (f32[3,1024,2]{1,2,0:T(2,128)S(1)}, f32[3,1024,2]{1,2,0:T(2,128)}, u32[]{:S(2)}) copy-start(f32[3,1024,2]{1,2,0:T(2,128)} %param.17) | copy-start | bytes 73732
  19.6 0.7 %copy-start.14 = (f32[4]{0:T(128)S(1)}, f32[4]{0:T(128)}, u32[]{:S(2)}) copy-start(f32[4]{0:T(128)} %param.23) | copy-start | bytes 52
  21.7 5.6 %collective-permute-start.6 = (f32[32,128]{1,0:T(8,128)S(1)}, f32[32,128]{1,0:T(8,128)S(1)}, u32[]{:S(2)}, u32[]{:S(2)}) collective-permute-start(f32[32,128]{1,0:T(8,128)S(1)} %shard_map.137.refs_0_), channel_id=1, source_target_pairs={{0,6},{2,4},{4,2},{6,0},{1,7},{3,5},{5,3},{7,1},{8,14},{10,12},{12... | collective-permute-start | bytes 49160 | tf_op jit(solution)/shard_map/ppermute | solution.py:42
  23.2 4.7 %collective-permute-start.5 = (f32[32,128]{1,0:T(8,128)S(1)}, f32[32,128]{1,0:T(8,128)S(1)}, u32[]{:S(2)}, u32[]{:S(2)}) collective-permute-start(f32[32,128]{1,0:T(8,128)S(1)} %shard_map.137.refs_0_), channel_id=1, source_target_pairs={{0,4},{2,6},{4,0},{6,2},{1,5},{3,7},{5,1},{7,3},{8,12},{10,14},{12... | collective-permute-start | bytes 49160 | tf_op jit(solution)/shard_map/ppermute | solution.py:42
  23.9 4.2 %collective-permute-start.4 = (f32[32,128]{1,0:T(8,128)S(1)}, f32[32,128]{1,0:T(8,128)S(1)}, u32[]{:S(2)}, u32[]{:S(2)}) collective-permute-start(f32[32,128]{1,0:T(8,128)S(1)} %shard_map.137.refs_0_), channel_id=1, source_target_pairs={{0,2},{2,0},{4,6},{6,4},{1,3},{3,1},{5,7},{7,5},{8,10},{10,8},{12,... | collective-permute-start | bytes 49160 | tf_op jit(solution)/shard_map/ppermute | solution.py:42
  28.0 1.2 %copy-start.3 = (bf16[1024,512]{1,0:T(8,128)(2,1)S(1)}, bf16[1024,512]{1,0:T(8,128)(2,1)}, u32[]{:S(2)}) copy-start(bf16[1024,512]{1,0:T(8,128)(2,1)} %refs_4_.4) | copy-start | bytes 3145732
  29.6 1.2 %collective-permute-start.7 = (bf16[3,512]{1,0:T(4,128)(2,1)S(1)}, bf16[3,512]{1,0:T(4,128)(2,1)S(1)}, u32[]{:S(2)}, u32[]{:S(2)}) collective-permute-start(bf16[3,512]{1,0:T(4,128)(2,1)S(1)} %shard_map.138.part), channel_id=1, source_target_pairs={{0,1},{1,0},{2,3},{3,2},{4,5},{5,4},{6,7},{7,6},{8,9},{9,8},{10,11... | collective-permute-start | bytes 9224 | tf_op jit(solution)/shard_map/ppermute | solution.py:42
  30.8 2.2 %copy-start = (bf16[512,4096]{1,0:T(8,128)(2,1)S(1)}, bf16[512,4096]{1,0:T(8,128)(2,1)}, u32[]{:S(2)}) copy-start(bf16[512,4096]{1,0:T(8,128)(2,1)} %w_up.1) | copy-start | bytes 12582916
  33.0 8.3 %copy-start.1 = (bf16[4096,512]{1,0:T(8,128)(2,1)S(1)}, bf16[4096,512]{1,0:T(8,128)(2,1)}, u32[]{:S(2)}) copy-start(bf16[4096,512]{1,0:T(8,128)(2,1)} %refs_4_.5) | copy-start | bytes 12582916
  33.7 6.1 %collective-permute-start.10 = (bf16[3,4224]{1,0:T(4,128)(2,1)S(1)}, bf16[3,4224]{1,0:T(4,128)(2,1)S(1)}, u32[]{:S(2)}, u32[]{:S(2)}) collective-permute-start(bf16[3,4224]{1,0:T(4,128)(2,1)S(1)} %get-tuple-element.10.refs_0_), channel_id=1, source_target_pairs={{0,6},{2,4},{4,2},{6,0},{1,7},{3,5},{5,3},{7,1},{8,14},{10,12},{12... | collective-permute-start | bytes 76040 | tf_op jit(solution)/shard_map/ppermute | solution.py:42
  36.1 4.8 %collective-permute-start.9 = (bf16[3,4224]{1,0:T(4,128)(2,1)S(1)}, bf16[3,4224]{1,0:T(4,128)(2,1)S(1)}, u32[]{:S(2)}, u32[]{:S(2)}) collective-permute-start(bf16[3,4224]{1,0:T(4,128)(2,1)S(1)} %get-tuple-element.10.refs_0_), channel_id=1, source_target_pairs={{0,4},{2,6},{4,0},{6,2},{1,5},{3,7},{5,1},{7,3},{8,12},{10,14},{12... | collective-permute-start | bytes 76040 | tf_op jit(solution)/shard_map/ppermute | solution.py:42
  37.0 4.3 %collective-permute-start.8 = (bf16[3,4224]{1,0:T(4,128)(2,1)S(1)}, bf16[3,4224]{1,0:T(4,128)(2,1)S(1)}, u32[]{:S(2)}, u32[]{:S(2)}) collective-permute-start(bf16[3,4224]{1,0:T(4,128)(2,1)S(1)} %get-tuple-element.10.refs_0_), channel_id=1, source_target_pairs={{0,2},{2,0},{4,6},{6,4},{1,3},{3,1},{5,7},{7,5},{8,10},{10,8},{12,... | collective-permute-start | bytes 76040 | tf_op jit(solution)/shard_map/ppermute | solution.py:42
  42.1 1.2 %collective-permute-start.11 = (bf16[3,256]{1,0:T(4,128)(2,1)S(1)}, bf16[3,256]{1,0:T(4,128)(2,1)S(1)}, u32[]{:S(2)}, u32[]{:S(2)}) collective-permute-start(bf16[3,256]{1,0:T(4,128)(2,1)S(1)} %get-tuple-element.12), channel_id=1, source_target_pairs={{0,1},{1,0},{2,3},{3,2},{4,5},{5,4},{6,7},{7,6},{8,9},{9,8},{10,11... | collective-permute-start | bytes 4616 | tf_op jit(solution)/shard_map/ppermute | solution.py:42
